TPU v7x, 32 devices: a whole 2x2x4 slice. The times are simulated.
32 devices in a mesh: sp: 8 (over z, x), tp: 4 (over y, core).
Axes of the slice: x: 2, y: 2, z: 4, core: 2. Of those that a mesh axis runs over, the one named last changes fastest.
Arguments:
- tokens: bfloat16 [4096, 4096], P(('sp', 'tp')), may hold values from -6 to 6
- lock_projector: bfloat16 [4096, 1024], P(None, 'tp'), may hold values from -0.01171875 to 0.01171875
- value_weight: bfloat16 [4096, 2048], P(None, 'tp'), may hold values from -0.0234375 to 0.0234375
- decay_weight: bfloat16 [4096, 1024], P(None, 'tp'), may hold values from -0.09375 to 0.09375
- decay_offset: float32 [1024], P('tp'), may hold values from -3.5 to 0
- fresh_question: bfloat16 [16, 64], P('tp'), may hold values from -6 to 6
Outputs:
- state_cache: bfloat16 [16, 64, 128], P('tp', 'sp')
- first_read: bfloat16 [16, 128], P('tp')
All inputs are finite; a program needn't handle non-finite values.
Results may differ from a plain program's by a relative error of at most 0.0034.
Values may be sent and summed in bfloat16 or wider, within the bound.
A program may use at most 64 MiB of HBM per device.

v0:
```python
import math

import jax
import jax.numpy as jnp
from jax import lax
from jax.sharding import PartitionSpec as P

CUE_WIDTH = 64
DV = 128


decay_tau = 16.0


def carried_in(part, axis, combine, identity):
    count = lax.axis_size(axis)
    place = lax.axis_index(axis)
    ahead = count - 1 - place
    gathered = lax.all_gather(part, axis)
    state = jnp.zeros_like(part) + jnp.asarray(identity, part.dtype)

    def one(hop, state):
        source = count - 1 - hop
        return combine(state, lax.dynamic_index_in_dim(gathered, source, 0, False))

    return lax.fori_loop(0, ahead, one, state)


def add_logs(earlier, later_sum):
    return earlier + later_sum


def per_device(tokens, lock_projector, value_weight, decay_weight, decay_offset, fresh_question):
    key_cols = lock_projector.shape[1]
    value_cols = value_weight.shape[1]
    local_heads = key_cols // CUE_WIDTH
    combined = jnp.concatenate([lock_projector, value_weight, decay_weight], axis=1)
    projected = jnp.dot(
        lax.all_gather(tokens, "tp", axis=0, tiled=True),
        combined,
        preferred_element_type=jnp.float32,
    )
    span_rows = projected.shape[0]
    lock_vectors = projected[:, :key_cols].astype(jnp.bfloat16)
    value_rows = projected[:, key_cols : key_cols + value_cols].astype(jnp.bfloat16)
    decay_pre = projected[:, key_cols + value_cols :]
    length = span_rows * lax.axis_size("sp")
    log_decay = jax.nn.log_sigmoid(decay_pre + decay_offset[None, :] + math.log(length)) / decay_tau
    segment_overall = jnp.sum(log_decay, axis=0)
    later_total = carried_in(segment_overall, "sp", add_logs, jnp.zeros_like(segment_overall))
    after = (segment_overall + later_total)[None, :] - jnp.cumsum(log_decay, axis=0)
    weighted = (lock_vectors.astype(jnp.float32) * jnp.exp(after)).astype(jnp.bfloat16)
    lookup_probes = weighted.reshape(span_rows, local_heads, CUE_WIDTH)
    stored_contents = value_rows.reshape(span_rows, local_heads, DV)
    summands_list = jnp.einsum(
        "nyl,nyp->ylp", lookup_probes, stored_contents, preferred_element_type=jnp.float32
    )
    key_scale = CUE_WIDTH ** (-0.5)
    question_widened = fresh_question.astype(jnp.float32)
    row_span = CUE_WIDTH // lax.axis_size("sp")
    row_start = lax.axis_index("sp") * row_span
    recall_grid = lax.psum(summands_list, "sp")
    segment_lines = lax.dynamic_slice_in_dim(recall_grid, row_start, row_span, 1)
    attended_blend = key_scale * jnp.einsum(
        "qw,qwi->qi", question_widened, recall_grid, precision=lax.Precision.HIGHEST
    )
    state_cache = segment_lines.astype(jnp.bfloat16)
    first_read = attended_blend * lax.rsqrt(
        jnp.mean(attended_blend * attended_blend, axis=-1, keepdims=True) + 1.0
    )
    return (state_cache, first_read.astype(jnp.bfloat16))


def solution(mesh):
    in_specs = (
        P(("sp", "tp"), None),
        P(None, "tp"),
        P(None, "tp"),
        P(None, "tp"),
        P("tp"),
        P("tp", None),
    )
    out_specs = (P("tp", "sp", None), P("tp", None))
    return jax.shard_map(
        per_device, mesh=mesh, in_specs=in_specs, out_specs=out_specs, check_vma=False
    )
```

profile of v0, /device:TPU:0, one launch (start us, length us, event | category | flops | bytes accessed | tf_op | source)
XLA Modules:
  0.0 155.6 jit_solution(18224980167365922461)
XLA Ops:
  7.2 0.0 copy-start
  7.2 0.0 all-gather.4.cloned.1.call-start
  7.2 0.7 all-gather.4.cloned.1.call-update
  7.9 0.0 all-reduce.2.cloned.1.call-start
  8.0 0.0 copy-start.1
  8.0 38.8 %all-gather.4.cloned.1.call-done = bf16[512,4096]{1,0:T(8,128)(2,1)} async-done(((bf16[128,4096]{1,0:T(8,128)(2,1)}), bf16[512,4096]{1,0:T(8,128)(2,1)}) %all-gather.4.cloned.1.call-update) | async-done | bytes 4194320 | tf_op jit(solution)/shard_map/all_gather | solution.py:39
  46.8 8.3 %fusion.22 = (bf16[512,1024]{0,1:T(8,128)(2,1)S(1)}, f32[512,1024]{0,1:T(8,128)S(1)}) fusion(bf16[512,4096]{1,0:T(8,128)(2,1)} %all-gather.4.cloned.1.call-done, bf16[4096,256]{1,0:T(8,128)(2,1)} %param.11, bf16[4096,512]{1,0:T(8,128)(2,1)} %param.10, bf16[4096,256]{1,0:T(8,128)(2,1)} %param.9), kind=kOutput, calls=%fused_computation.31 | convolution fusion | flops 4320657408 | bytes 15728640 | tf_op jit(solution)/shard_map/dot_general | solution.py:38
  55.1 0.0 copy-done.1
  55.1 0.5 fusion.21
  55.6 20.5 %all-gather.1 = f32[8,1,256]{2,1,0:T(1,128)S(1)} all-gather(f32[1,1,256]{2,1,0:T(1,128)S(1)} %bitcast.54), channel_id=2, replica_groups=mesh['sp'=8,'tp'=4] {'sp'}, dimensions={0}, use_global_device_ids=true | all-gather | bytes 9216 | tf_op jit(solution)/shard_map/all_gather | solution.py:19
  76.1 0.3 while.12
  76.5 0.2 reshape.30
  76.7 0.2 copy.11
  76.9 0.1 fusion.23
  77.2 0.3 copy.12
  77.5 0.2 fusion.14
  77.6 1.0 fusion.24
  78.6 0.0 all-reduce.2.cloned.1.call-update
  78.6 67.0 %all-reduce.2.cloned.1.call-done = f32[4,64,128]{2,1,0:T(8,128)} async-done(((f32[4,64,128]{2,1,0:T(8,128)}), f32[4,64,128]{2,1,0:T(8,128)}) %all-reduce.2.cloned.1.call-update) | async-done | bytes 131088 | tf_op jit(solution)/shard_map/psum | solution.py:62
  145.6 0.0 copy-done
  145.6 1.1 fusion.17
  146.7 0.1 multiply_reduce_fusion
  146.8 0.6 multiply_convert_fusion
  147.5 1.3 dynamic-slice_convert_fusion
  (24 shorter events, 0.3 us)
Async XLA Ops:
  7.2 138.4 %copy-start = (bf16[4,64]{1,0:T(4,128)(2,1)S(1)}, bf16[4,64]{1,0:T(4,128)(2,1)}, u32[]{:S(2)}) copy-start(bf16[4,64]{1,0:T(4,128)(2,1)} %param.13) | copy-start | bytes 1540
  7.2 39.6 %all-gather.4.cloned.1.call-start = ((), (), s32[]{:S(2)}) async-start(), calls=%async_computation | async-start | bytes 5242880 | tf_op jit(solution)/shard_map/all_gather | solution.py:39
  7.9 137.7 %all-reduce.2.cloned.1.call-start = ((), (), s32[]{:S(2)}) async-start(), calls=%async_computation.1 | async-start | bytes 262144 | tf_op jit(solution)/shard_map/psum | solution.py:62
  8.0 47.1 %copy-start.1 = (f32[256]{0:T(256)S(1)}, f32[256]{0:T(256)}, u32[]{:S(2)}) copy-start(f32[256]{0:T(256)} %param.12) | copy-start | bytes 3076
Sparse Core Ops, SparseCore 0:
  9.5 37.1 all-gather.3
  78.7 66.8 all-reduce.1
where the time goes:
time: 156 us
  waiting for transfers between devices  106 us (68%)
  blocking collectives  20.5 us (13%)
  between operations  14.1 us (9%)
  matrix products  10.3 us (7%)
  local copies, waits for them, and re-layouts  2.13 us (1%)
  other arithmetic  1.74 us (1%)
    psum x1, waiting for transfers between devices, per_device(): recall_grid = lax.psum(summands_list, 'sp')  67 us
    all_gather x1, waiting for transfers between devices, per_device(): lax.all_gather(tokens, 'tp', axis=0, tiled=True)  38.8 us
    all_gather x1, blocking collectives, carried_in(): gathered = lax.all_gather(part, axis)  20.5 us
    dot_general x1, matrix products, per_device(): jnp.dot(lax.all_gather(tokens, 'tp', axis=0, tiled=True), combined, prefe...  8.32 us
  transfers between devices with their start and end apart: 2, of which 2 were waited for; matrix products, arithmetic and copies ran while one was open for 0% of the time, Pallas kernels for 0%

commit v1 on v0

v1 whole, which is shorter than its diff:
```python
import functools
import math

import jax
import jax.numpy as jnp
from jax import lax
from jax.experimental import pallas as pl
from jax.experimental.pallas import tpu as pltpu
from jax.sharding import PartitionSpec as P

DECAY_TAU = 16.0
CORES = 2
LANES = 128
MESH = pl.DeviceIdType.MESH


def kernel(
    n_sp, n_tp, chunks,
    tokens, w_key, w_value, w_decay, offset, question,
    cache_out, read_out,
    x_buf, key_buf, value_buf, decay_buf, key_acc, value_acc, decay_acc,
    log_buf, pair_total, spread_q, total_send, total_recv, state_send, state_recv,
    token_sem, weight_sem, y_send, y_recv, d_send, d_recv, t_send, t_recv, s_send, s_recv,
):
    rows, width = tokens.shape
    key_cols = w_key.shape[1]
    heads, cue = question.shape
    dv = w_value.shape[1] // heads
    depth = width // chunks
    pairs = n_tp // CORES
    pair_rows = CORES * rows
    row_span = cue // n_sp
    lanes_padded = total_send.shape[-1]
    length = rows * n_tp * n_sp

    sp = lax.axis_index("sp")
    tp = lax.axis_index("tp")
    pair = tp // CORES
    core = lax.rem(tp, CORES)
    partner = pair * CORES + (1 - core)

    def pair_at(i):
        return lax.rem(pair + pairs - i, pairs)

    def token_copy(c):
        start = c * depth if isinstance(c, int) else pl.multiple_of(c * depth, depth)
        return pltpu.make_async_copy(
            tokens.at[:, pl.ds(start, depth)], x_buf.at[c, pair, core], token_sem.at[c]
        )

    def weight_copies(c):
        start = c * depth if isinstance(c, int) else pl.multiple_of(c * depth, depth)
        return [
            pltpu.make_async_copy(w.at[pl.ds(start, depth), :], b.at[c], weight_sem.at[n, c])
            for n, (w, b) in enumerate(
                ((w_decay, decay_buf), (w_key, key_buf), (w_value, value_buf))
            )
        ]

    def across_send(i, c):
        to = lax.rem(pair + i, pairs) * CORES + core
        block = x_buf.at[c, pair, core]
        return pltpu.make_async_remote_copy(
            block, block, y_send.at[i, c], y_recv.at[i, c], device_id={"tp": to}, device_id_type=MESH
        )

    def across_recv(i, c):
        block = x_buf.at[c, pair_at(i), core]
        return pltpu.make_async_remote_copy(
            block, block, y_send.at[i, c], y_recv.at[i, c],
            device_id={"tp": pair_at(i) * CORES + core}, device_id_type=MESH,
        )

    def beside(i, c, which):
        block = x_buf.at[c, pair_at(i), which]
        return pltpu.make_async_remote_copy(
            block, block, d_send.at[i, c], d_recv.at[i, c],
            device_id={"tp": partner}, device_id_type=MESH,
        )

    def total_copy(i, slot):
        return pltpu.make_async_remote_copy(
            total_send, total_recv.at[slot], t_send.at[i], t_recv.at[i],
            device_id={"sp": lax.rem(sp + i, n_sp)}, device_id_type=MESH,
        )

    def state_copy(i, slot):
        to = lax.rem(sp + i, n_sp)
        return pltpu.make_async_remote_copy(
            state_send.at[to], state_recv.at[slot], s_send.at[i], s_recv.at[i],
            device_id={"sp": to}, device_id_type=MESH,
        )

    for c in range(chunks):
        token_copy(c).start()
    for c in range(chunks):
        for copy in weight_copies(c):
            copy.start()

    barrier = pltpu.get_barrier_semaphore()
    pl.semaphore_signal(barrier, inc=1, device_id={"tp": partner}, device_id_type=MESH)
    for i in range(1, pairs):
        pl.semaphore_signal(
            barrier, inc=1,
            device_id={"tp": lax.rem(pair + i, pairs) * CORES + core}, device_id_type=MESH,
        )
    for i in range(1, n_sp):
        pl.semaphore_signal(
            barrier, inc=1, device_id={"sp": lax.rem(sp + i, n_sp)}, device_id_type=MESH
        )

    wide_q = question[...].astype(jnp.float32)
    eye = lax.broadcasted_iota(jnp.int32, (cue, cue), 0) == lax.broadcasted_iota(
        jnp.int32, (cue, cue), 1
    )
    ones = jnp.ones((cue, dv), jnp.bfloat16)
    for h in range(heads):
        diagonal = jnp.where(eye, jnp.broadcast_to(wide_q[h : h + 1, :], (cue, cue)), 0.0)
        spread_q[h] = jnp.dot(
            diagonal.astype(jnp.bfloat16), ones, preferred_element_type=jnp.float32
        )

    pl.semaphore_wait(barrier, 1 + (pairs - 1) + (n_sp - 1))

    for c in range(chunks):
        token_copy(c).wait()
        for i in range(1, pairs):
            across_send(i, c).start()
        beside(0, c, core).start()

    def product(p, c, buf, acc, first):
        x = x_buf[c, p].reshape(pair_rows, depth)
        out = jnp.dot(x, buf[c], preferred_element_type=jnp.float32)
        if first:
            acc[p] = out
        else:
            acc[p] += out

    def all_products(p, c, first):
        product(p, c, decay_buf, decay_acc, first)
        product(p, c, key_buf, key_acc, first)
        product(p, c, value_buf, value_acc, first)

    def finish_decay(p):
        pre = decay_acc[p] + offset[...] + math.log(length)
        log_decay = (jnp.minimum(pre, 0.0) - jnp.log1p(jnp.exp(-jnp.abs(pre)))) / DECAY_TAU
        log_buf[p] = log_decay
        pair_total[p] = jnp.sum(log_decay, axis=0, keepdims=True)

    def send_totals():
        whole = pair_total[0]
        for p in range(1, pairs):
            whole = whole + pair_total[p]
        if lanes_padded > key_cols:
            whole = jnp.concatenate(
                [whole, jnp.zeros((1, lanes_padded - key_cols), jnp.float32)], axis=1
            )
        total_send[...] = whole
        total_recv[sp] = whole
        for i in range(1, n_sp):
            total_copy(i, sp).start()

    def arrive(i, c):
        if i == 0:
            for copy in weight_copies(c):
                copy.wait()
        else:
            across_recv(i, c).wait_recv()
            beside(i, c, core).start()

    for i in range(pairs):
        p = pair_at(i)
        arrive(i, 0)
        arrive(i, 1)
        beside(i, 0, 1 - core).wait_recv()
        all_products(p, 0, True)

        def step(c, carry, i=i, p=p):
            arrive(i, c + 1)
            beside(i, c, 1 - core).wait_recv()
            all_products(p, c, False)
            return carry

        lax.fori_loop(1, chunks - 1, step, 0)
        last = chunks - 1
        beside(i, last, 1 - core).wait_recv()
        product(p, last, decay_buf, decay_acc, False)
        finish_decay(p)
        if i == pairs - 1:
            send_totals()
        product(p, last, key_buf, key_acc, False)
        product(p, last, value_buf, value_acc, False)

    later = lax.broadcasted_iota(jnp.int32, (pair_rows, pair_rows), 1) > lax.broadcasted_iota(
        jnp.int32, (pair_rows, pair_rows), 0
    )
    later = jnp.where(later, 1.0, 0.0).astype(jnp.bfloat16)
    group = 2 if heads % 2 == 0 else 1
    gk, gv = group * cue, group * dv
    sums = [None] * (heads // group)
    behind = jnp.zeros((1, key_cols), jnp.float32)
    for p in reversed(range(pairs)):
        log_decay = log_buf[p]
        after = behind
        rest = log_decay
        for _ in range(3):
            part = rest.astype(jnp.bfloat16)
            rest = rest - part.astype(jnp.float32)
            after = after + jnp.dot(later, part, preferred_element_type=jnp.float32)
        behind = behind + pair_total[p]
        keys = key_acc[p].astype(jnp.bfloat16).astype(jnp.float32)
        weighted = (keys * jnp.exp(after)).astype(jnp.bfloat16)
        values = value_acc[p].astype(jnp.bfloat16)
        for g in range(heads // group):
            term = lax.dot_general(
                weighted[:, g * gk : (g + 1) * gk],
                values[:, g * gv : (g + 1) * gv],
                (((0,), (0,)), ((), ())),
                preferred_element_type=jnp.float32,
            )
            sums[g] = term if sums[g] is None else sums[g] + term

    for i in range(1, n_sp):
        total_copy(i, lax.rem(sp + n_sp - i, n_sp)).wait_recv()
    later_total = jnp.zeros((1, lanes_padded), jnp.float32)
    for s in range(n_sp):
        later_total = later_total + jnp.where(sp < s, total_recv[s], 0.0)
    kept = jnp.exp(later_total)
    base = heads * row_span
    for g in range(heads // group):
        lo = g * gk // LANES * LANES
        turned = jnp.broadcast_to(kept[:, lo : lo + LANES], (LANES, LANES)).T
        for j in range(group):
            h = g * group + j
            at = h * cue - lo
            spread = turned[at : at + cue]
            if dv != LANES:
                spread = jnp.broadcast_to(spread[:, :1], (cue, dv))
            state = sums[g][j * cue : (j + 1) * cue, j * dv : (j + 1) * dv] * spread
            heard = jnp.sum(state * spread_q[h], axis=0, keepdims=True) * cue**-0.5
            for s in range(n_sp):
                state_send[s, h * row_span : (h + 1) * row_span, :] = state[
                    s * row_span : (s + 1) * row_span
                ]
                state_send[s, base + h : base + h + 1, :] = heard
    for i in range(1, n_sp):
        state_copy(i, sp).start()
    state_recv[sp] = state_send[sp]
    for i in range(1, n_sp):
        state_copy(i, lax.rem(sp + n_sp - i, n_sp)).wait_recv()
    total = state_recv[0]
    for s in range(1, n_sp):
        total = total + state_recv[s]
    for h in range(heads):
        cache_out[h] = total[h * row_span : (h + 1) * row_span].astype(jnp.bfloat16)
    heard = total[base : base + heads]
    scale = lax.rsqrt(jnp.mean(heard * heard, axis=-1, keepdims=True) + 1.0)
    read_out[...] = (heard * scale).astype(jnp.bfloat16)

    def drain(c, carry):
        for i in range(1, pairs):
            across_send(i, c).wait_send()
        for i in range(pairs):
            beside(i, c, core).wait_send()
        return carry

    lax.fori_loop(0, chunks, drain, 0)
    for i in range(1, n_sp):
        total_copy(i, sp).wait_send()
        state_copy(i, sp).wait_send()


def per_device(n_sp, n_tp, tokens, lock_projector, value_weight, decay_weight, decay_offset, fresh_question):
    rows, width = tokens.shape
    key_cols = lock_projector.shape[1]
    value_cols = value_weight.shape[1]
    heads, cue = fresh_question.shape
    dv = value_cols // heads
    row_span = cue // n_sp
    pairs = n_tp // CORES
    chunks = 8
    depth = width // chunks
    lanes_padded = max(key_cols, LANES)
    message = -(-(heads * row_span + heads) // 8) * 8
    f32, bf16 = jnp.float32, jnp.bfloat16
    dma = pltpu.SemaphoreType.DMA
    any_spec = pl.BlockSpec(memory_space=pl.ANY)
    vmem_spec = pl.BlockSpec(memory_space=pltpu.VMEM)
    pair_rows = CORES * rows
    return pl.pallas_call(
        functools.partial(kernel, n_sp, n_tp, chunks),
        out_shape=(
            jax.ShapeDtypeStruct((heads, row_span, dv), bf16),
            jax.ShapeDtypeStruct((heads, dv), bf16),
        ),
        in_specs=[any_spec] * 4 + [vmem_spec] * 2,
        out_specs=(vmem_spec, vmem_spec),
        scratch_shapes=[
            pltpu.VMEM((chunks, pairs, CORES, rows, depth), bf16),
            pltpu.VMEM((chunks, depth, key_cols), bf16),
            pltpu.VMEM((chunks, depth, value_cols), bf16),
            pltpu.VMEM((chunks, depth, key_cols), bf16),
            pltpu.VMEM((pairs, pair_rows, key_cols), f32),
            pltpu.VMEM((pairs, pair_rows, value_cols), f32),
            pltpu.VMEM((pairs, pair_rows, key_cols), f32),
            pltpu.VMEM((pairs, pair_rows, key_cols), f32),
            pltpu.VMEM((pairs, 1, key_cols), f32),
            pltpu.VMEM((heads, cue, dv), f32),
            pltpu.VMEM((1, lanes_padded), f32),
            pltpu.VMEM((n_sp, 1, lanes_padded), f32),
            pltpu.VMEM((n_sp, message, dv), f32),
            pltpu.VMEM((n_sp, message, dv), f32),
            dma((chunks,)),
            dma((3, chunks)),
            dma((pairs, chunks)),
            dma((pairs, chunks)),
            dma((pairs, chunks)),
            dma((pairs, chunks)),
            dma((n_sp,)),
            dma((n_sp,)),
            dma((n_sp,)),
            dma((n_sp,)),
        ],
        compiler_params=pltpu.CompilerParams(
            collective_id=0, has_side_effects=True, vmem_limit_bytes=60 * 1024 * 1024
        ),
        name="gated_state",
    )(
        tokens, lock_projector, value_weight, decay_weight,
        decay_offset.reshape(1, key_cols), fresh_question,
    )


def solution(mesh):
    in_specs = (
        P(("sp", "tp"), None),
        P(None, "tp"),
        P(None, "tp"),
        P(None, "tp"),
        P("tp"),
        P("tp", None),
    )
    out_specs = (P("tp", "sp", None), P("tp", None))
    body = functools.partial(per_device, mesh.shape["sp"], mesh.shape["tp"])
    return jax.shard_map(body, mesh=mesh, in_specs=in_specs, out_specs=out_specs, check_vma=False)
```

time: 156 us -> 46.2 us (0.30)
  waiting for transfers between devices: 106 us -> 0 us
  Pallas kernels: 0 us -> 42.8 us
  blocking collectives: 20.5 us -> 0 us
  between operations: 14.1 us -> 0.64 us
  matrix products: 10.3 us -> 0 us
  other arithmetic: 1.74 us -> 0 us
    psum x1 -> x0, waiting for transfers between devices: 67 us -> none  [per_device(): recall_grid = lax.psum(summands_list, 'sp')]
    pallas_call x0 -> x1, Pallas kernels: none -> 42.8 us  [per_device(): pl.pallas_call(functools.partial(kernel, n_sp, n_tp, chunks), out_shape=(...]
    all_gather x1 -> x0, waiting for transfers between devices: 38.8 us -> none  [per_device(): lax.all_gather(tokens, 'tp', axis=0, tiled=True)]
    all_gather x1 -> x0, blocking collectives: 20.5 us -> none  [carried_in(): gathered = lax.all_gather(part, axis)]
    dot_general x3 -> x0, matrix products: 10.3 us -> none  [the longest x1 8.32 us: per_device(): jnp.dot(lax.all_gather(tokens, 'tp', axis=0, tiled=True), combined, prefe...]
    unnamed x6 -> x2, local copies, waits for them, and re-layouts: 0.02 us -> 2.51 us
  transfers between devices with their start and end apart: 2 -> 0, of which waited for: 2 -> 0; matrix products, arithmetic and copies ran while one was open for 0% -> 0% of each run, Pallas kernels for 0% -> 0%
where the time goes in v1:
time: 46.2 us; the launch traced here: 45.9 us
  Pallas kernels  42.8 us (93%)
  local copies, waits for them, and re-layouts  2.51 us (5%)
  between operations  0.64 us (1%)
    pallas_call x1, Pallas kernels, per_device(): pl.pallas_call(functools.partial(kernel, n_sp, n_tp, chunks), out_shape=(...  42.8 us
    unnamed x2, local copies, waits for them, and re-layouts  2.51 us

profile of v1, /device:TPU:0, one launch (start us, length us, event | category | flops | bytes accessed | tf_op | source)
XLA Modules:
  0.0 45.9 jit_solution(2655831596598400323)
XLA Ops:
  0.6 42.8 %gated_state.1 = (bf16[4,8,128]{2,1,0:T(8,128)(2,1)}, bf16[4,128]{1,0:T(4,128)(2,1)}) custom-call(bf16[128,4096]{1,0:T(8,128)(2,1)} %tokens.1, bf16[4096,256]{1,0:T(8,128)(2,1)} %w_key.1, bf16[4096,512]{1,0:T(8,128)(2,1)} %w_value.1, bf16[4096,256]{1,0:T(8,128)(2,1)} %w_decay.1, f32[1,256]{1,0:T(1,128)} %bitcast.1, bf16[4,64]{1,0:T(4,128)(2,1)} %question.1), custom_call_target="tpu_custom_call" | custom-call | tf_op jit(solution)/shard_map/gated_state/pallas_call | solution.py:290
  43.4 1.3 %copy.10 = bf16[4,8,128]{2,1,0:T(8,128)(2,1)} copy(bf16[4,8,128]{2,1,0:T(8,128)(2,1)} %get-tuple-element.4) | data formatting | bytes 16384
  44.7 1.2 %copy.11 = bf16[4,128]{1,0:T(4,128)(2,1)} copy(bf16[4,128]{1,0:T(4,128)(2,1)} %get-tuple-element.5) | data formatting | bytes 2048

commit v2 on v1

--- a/solution.py
+++ b/solution.py
@@ -17,7 +17,7 @@
 def kernel(
     n_sp, n_tp, chunks,
     tokens, w_key, w_value, w_decay, offset, question,
-    cache_out, read_out,
+    total_out,
     x_buf, key_buf, value_buf, decay_buf, key_acc, value_acc, decay_acc,
     log_buf, pair_total, spread_q, total_send, total_recv, state_send, state_recv,
     token_sem, weight_sem, y_send, y_recv, d_send, d_recv, t_send, t_recv, s_send, s_recv,
@@ -209,16 +209,19 @@
             after = after + jnp.dot(later, part, preferred_element_type=jnp.float32)
         behind = behind + pair_total[p]
         keys = key_acc[p].astype(jnp.bfloat16).astype(jnp.float32)
-        weighted = (keys * jnp.exp(after)).astype(jnp.bfloat16)
+        exact = keys * jnp.exp(after)
+        upper = exact.astype(jnp.bfloat16)
+        lower = (exact - upper.astype(jnp.float32)).astype(jnp.bfloat16)
         values = value_acc[p].astype(jnp.bfloat16)
         for g in range(heads // group):
-            term = lax.dot_general(
-                weighted[:, g * gk : (g + 1) * gk],
-                values[:, g * gv : (g + 1) * gv],
-                (((0,), (0,)), ((), ())),
-                preferred_element_type=jnp.float32,
-            )
-            sums[g] = term if sums[g] is None else sums[g] + term
+            for weighted in (upper, lower):
+                term = lax.dot_general(
+                    weighted[:, g * gk : (g + 1) * gk],
+                    values[:, g * gv : (g + 1) * gv],
+                    (((0,), (0,)), ((), ())),
+                    preferred_element_type=jnp.float32,
+                )
+                sums[g] = term if sums[g] is None else sums[g] + term
 
     for i in range(1, n_sp):
         total_copy(i, lax.rem(sp + n_sp - i, n_sp)).wait_recv()
@@ -251,11 +254,7 @@
     total = state_recv[0]
     for s in range(1, n_sp):
         total = total + state_recv[s]
-    for h in range(heads):
-        cache_out[h] = total[h * row_span : (h + 1) * row_span].astype(jnp.bfloat16)
-    heard = total[base : base + heads]
-    scale = lax.rsqrt(jnp.mean(heard * heard, axis=-1, keepdims=True) + 1.0)
-    read_out[...] = (heard * scale).astype(jnp.bfloat16)
+    total_out[...] = total
 
     def drain(c, carry):
         for i in range(1, pairs):
@@ -268,6 +267,14 @@
     for i in range(1, n_sp):
         total_copy(i, sp).wait_send()
         state_copy(i, sp).wait_send()
+
+
+def finish(heads, row_span, total, cache_out, read_out):
+    for h in range(heads):
+        cache_out[h] = total[h * row_span : (h + 1) * row_span, :].astype(jnp.bfloat16)
+    heard = total[heads * row_span : heads * (row_span + 1), :]
+    scale = lax.rsqrt(jnp.mean(heard * heard, axis=-1, keepdims=True) + 1.0)
+    read_out[...] = (heard * scale).astype(jnp.bfloat16)
 
 
 def per_device(n_sp, n_tp, tokens, lock_projector, value_weight, decay_weight, decay_offset, fresh_question):
@@ -287,14 +294,11 @@
     any_spec = pl.BlockSpec(memory_space=pl.ANY)
     vmem_spec = pl.BlockSpec(memory_space=pltpu.VMEM)
     pair_rows = CORES * rows
-    return pl.pallas_call(
+    total = pl.pallas_call(
         functools.partial(kernel, n_sp, n_tp, chunks),
-        out_shape=(
-            jax.ShapeDtypeStruct((heads, row_span, dv), bf16),
-            jax.ShapeDtypeStruct((heads, dv), bf16),
-        ),
+        out_shape=jax.ShapeDtypeStruct((message, dv), f32),
         in_specs=[any_spec] * 4 + [vmem_spec] * 2,
-        out_specs=(vmem_spec, vmem_spec),
+        out_specs=vmem_spec,
         scratch_shapes=[
             pltpu.VMEM((chunks, pairs, CORES, rows, depth), bf16),
             pltpu.VMEM((chunks, depth, key_cols), bf16),
@@ -329,6 +333,16 @@
         tokens, lock_projector, value_weight, decay_weight,
         decay_offset.reshape(1, key_cols), fresh_question,
     )
+    return pl.pallas_call(
+        functools.partial(finish, heads, row_span),
+        out_shape=(
+            jax.ShapeDtypeStruct((heads, row_span, dv), bf16),
+            jax.ShapeDtypeStruct((heads, dv), bf16),
+        ),
+        in_specs=[vmem_spec],
+        out_specs=(vmem_spec, vmem_spec),
+        name="finish",
+    )(total)
 
 
 def solution(mesh):

time: 46.2 us -> 44.9 us (0.972)
  local copies, waits for them, and re-layouts: 2.51 us -> 0 us
  Pallas kernels: 42.8 us -> 44.1 us
    unnamed x2 -> x0, local copies, waits for them, and re-layouts: 2.51 us -> none
    pallas_call x1 -> x2, Pallas kernels: 42.8 us -> 44.1 us  [the longest x1 42.7 us: per_device(): pl.pallas_call(functools.partial(kernel, n_sp, n_tp, chunks), out_shape=j...]
where the time goes in v2:
time: 44.9 us; the launch traced here: 44.7 us
  Pallas kernels  44.1 us (98%)
  between operations  0.64 us (1%)
    pallas_call x1, Pallas kernels, per_device(): pl.pallas_call(functools.partial(kernel, n_sp, n_tp, chunks), out_shape=j...  42.7 us
    pallas_call x1, Pallas kernels, per_device(): pl.pallas_call(functools.partial(finish, heads, row_span), out_shape=(jax...  1.38 us

profile of v2, /device:TPU:0, one launch (start us, length us, event | category | flops | bytes accessed | tf_op | source)
XLA Modules:
  0.0 44.7 jit_solution(8863656732318946164)
XLA Ops:
  0.6 42.7 %gated_state.1.total = f32[40,128]{1,0:T(8,128)} custom-call(bf16[128,4096]{1,0:T(8,128)(2,1)} %tokens.1, bf16[4096,256]{1,0:T(8,128)(2,1)} %w_key.1, bf16[4096,512]{1,0:T(8,128)(2,1)} %w_value.1, bf16[4096,256]{1,0:T(8,128)(2,1)} %w_decay.1, f32[1,256]{1,0:T(1,128)} %bitcast.1, bf16[4,64]{1,0:T(4,128)(2,1)} %question.1), custom_call_target="tpu_custom_call" | custom-call | tf_op jit(solution)/shard_map/gated_state/pallas_call | solution.py:297
  43.3 1.4 %finish.1 = (bf16[4,8,128]{2,1,0:T(8,128)(2,1)}, bf16[4,128]{1,0:T(4,128)(2,1)}) custom-call(f32[40,128]{1,0:T(8,128)} %gated_state.1.total), custom_call_target="tpu_custom_call" | custom-call | tf_op jit(solution)/shard_map/finish/pallas_call | solution.py:336

commit v3 on v2

--- a/solution.py
+++ b/solution.py
@@ -126,6 +126,7 @@
         token_copy(c).wait()
         for i in range(1, pairs):
             across_send(i, c).start()
+    for c in range(chunks):
         beside(0, c, core).start()
 
     def product(p, c, buf, acc, first):
@@ -285,10 +286,10 @@
     dv = value_cols // heads
     row_span = cue // n_sp
     pairs = n_tp // CORES
-    chunks = 8
+    chunks = 4
     depth = width // chunks
     lanes_padded = max(key_cols, LANES)
-    message = -(-(heads * row_span + heads) // 8) * 8
+    message = heads * row_span + heads
     f32, bf16 = jnp.float32, jnp.bfloat16
     dma = pltpu.SemaphoreType.DMA
     any_spec = pl.BlockSpec(memory_space=pl.ANY)

time: 44.9 us -> 44.6 us (level)
  no operation moved by 1% of the time
where the time goes in v3:
time: 44.6 us; the launch traced here: 44.4 us
  Pallas kernels  43.7 us (98%)
  between operations  0.64 us (1%)
    pallas_call x1, Pallas kernels, per_device(): pl.pallas_call(functools.partial(kernel, n_sp, n_tp, chunks), out_shape=j...  42.4 us
    pallas_call x1, Pallas kernels, per_device(): pl.pallas_call(functools.partial(finish, heads, row_span), out_shape=(jax...  1.38 us

profile of v3, /device:TPU:0, one launch (start us, length us, event | category | flops | bytes accessed | tf_op | source)
XLA Modules:
  0.0 44.4 jit_solution(6590834650814467646)
XLA Ops:
  0.6 42.4 %gated_state.1.total = f32[36,128]{1,0:T(8,128)} custom-call(bf16[128,4096]{1,0:T(8,128)(2,1)} %tokens.1, bf16[4096,256]{1,0:T(8,128)(2,1)} %w_key.1, bf16[4096,512]{1,0:T(8,128)(2,1)} %w_value.1, bf16[4096,256]{1,0:T(8,128)(2,1)} %w_decay.1, f32[1,256]{1,0:T(1,128)} %bitcast.1, bf16[4,64]{1,0:T(4,128)(2,1)} %question.1), custom_call_target="tpu_custom_call" | custom-call | tf_op jit(solution)/shard_map/gated_state/pallas_call | solution.py:298
  43.0 1.4 %finish.1 = (bf16[4,8,128]{2,1,0:T(8,128)(2,1)}, bf16[4,128]{1,0:T(4,128)(2,1)}) custom-call(f32[36,128]{1,0:T(8,128)} %gated_state.1.total), custom_call_target="tpu_custom_call" | custom-call | tf_op jit(solution)/shard_map/finish/pallas_call | solution.py:337
